TPU v7x, 32 devices: a whole 2x2x4 slice. The times are simulated.
32 devices in a mesh: sp: 16 (over z, y, x), tp: 2 (over core).
Axes of the slice: x: 2, y: 2, z: 4, core: 2. Of those that a mesh axis runs over, the one named last changes fastest.
Arguments:
- resid: bfloat16 [6144, 2048], P('sp', 'tp'), may hold values from -40 to 40
- query_one: bfloat16 [6144, 1024], P('sp', 'tp'), may hold values from -64 to 64
- key_one: bfloat16 [6144, 1024], P('sp', 'tp'), may hold values from -64 to 64
- query_two: bfloat16 [6144, 1024], P('sp', 'tp'), may hold values from -64 to 64
- key_two: bfloat16 [6144, 1024], P('sp', 'tp'), may hold values from -64 to 64
- values: bfloat16 [6144, 2048], P('sp', 'tp'), may hold values from -6 to 6
- mix_lambda: float32 [8], P('tp'), may hold values from 0.3 to 0.8
- segments: int32 [6144], P('sp'), may hold values from 0 to 7, never falling along the last dimension, each value on 1 to 1536 neighbouring positions
- head_gain: float32 [256], replicated, may hold values from 0.1 to 1.9
- out_weight: bfloat16 [2048, 2048], P(None, 'tp'), may hold values from -0.125 to 0.125
- mixer_gain: float32 [2048], P('tp'), may hold values from 0.1 to 1.9
- gate_weight: bfloat16 [2048, 6144], P('sp', 'tp'), may hold values from -0.125 to 0.125
- up_weight: bfloat16 [2048, 6144], P('sp', 'tp'), may hold values from -0.125 to 0.125
- down_weight: bfloat16 [6144, 2048], P('tp', 'sp'), may hold values from -0.078125 to 0.078125
Outputs:
- layer_out: bfloat16 [6144, 2048], P('sp', 'tp')
Inputs may be any that keep to these rules, and one draw needn't show every extreme that they name: `segments`: numbers never fall along the sequence; each document has at most 1536 positions and one has exactly that many.
All inputs are finite; a program needn't handle non-finite values.
Results may differ from a plain program's by a relative error of at most 0.012.
Values may be sent and summed in bfloat16 or wider, within the bound.
A program may use at most 128 MiB of HBM per device.

v0:
```python
import jax
import jax.numpy as jnp
from jax import lax
from jax.sharding import PartitionSpec as P

HD = 128
VD = 256
REACH = 4
SHARE = 2


def shifted(value, axis, by):
    length = lax.axis_size(axis)
    pairs = [(i, i + by) for i in range(length) if 0 <= i + by < length]
    return lax.ppermute(value, axis, pairs)


def groups(length):
    share = SHARE if length % SHARE == 0 else 1
    plane = [[i * share + j for j in range(share)] for i in range(length // share)]
    across = [[i * share + j for i in range(length // share)] for j in range(share)]
    return plane, across


def spread(blocks):
    length = lax.axis_size("sp")
    share = blocks.shape[0]
    if share == 1:
        return blocks
    mine = lax.rem(lax.axis_index("sp"), share)
    own = lax.dynamic_index_in_dim(blocks, mine, 0, keepdims=True)
    result = lax.dynamic_update_slice_in_dim(jnp.zeros_like(blocks), own, mine, 0)
    for by in range(1, share):
        pairs = [(i, i - i % share + (i + by) % share) for i in range(length)]
        sent = lax.dynamic_index_in_dim(blocks, lax.rem(mine + by, share), 0, keepdims=True)
        came = lax.ppermute(sent, "sp", pairs)
        result = lax.dynamic_update_slice_in_dim(result, came, lax.rem(mine + share - by, share), 0)
    return result


def gathered(gate_weight, up_weight, down_weight):
    plane, across = groups(lax.axis_size("sp"))
    share = len(plane[0])
    depth, units = gate_weight.shape
    part = units // share
    both = [gate_weight.reshape(depth, share, part), up_weight.reshape(depth, share, part)]
    both = jnp.concatenate(both, 2).transpose(1, 0, 2)
    both = spread(both).reshape(share * depth, 2 * part)
    down = spread(down_weight.reshape(share, part, depth))
    down = down.transpose(1, 0, 2).reshape(part, share * depth)
    both = lax.all_gather(both, "sp", axis=0, tiled=True, axis_index_groups=across)
    down = lax.all_gather(down, "sp", axis=1, tiled=True, axis_index_groups=across)
    return both, down


def swapped(value, axis, members):
    return lax.ppermute(value, axis, [(i, i ^ 1) for i in range(members)])


def whole_channels(value):
    members = lax.axis_size("tp")
    if members != 2:
        return lax.all_gather(value, "tp", axis=1, tiled=True)
    other = swapped(value, "tp", members)
    mine = lax.axis_index("tp") * value.shape[1]
    result = jnp.zeros((value.shape[0], 2 * value.shape[1]), value.dtype)
    result = lax.dynamic_update_slice_in_dim(result, value, mine, 1)
    return lax.dynamic_update_slice_in_dim(result, other, value.shape[1] - mine, 1)


def own_channels(terms):
    members = lax.axis_size("tp")
    if members != 2:
        return lax.psum_scatter(terms, "tp", scatter_dimension=1, tiled=True).astype(jnp.float32)
    width = terms.shape[1] // 2
    mine = lax.axis_index("tp") * width
    other = swapped(lax.dynamic_slice_in_dim(terms, width - mine, width, 1), "tp", members)
    own = lax.dynamic_slice_in_dim(terms, mine, width, 1)
    return own.astype(jnp.float32) + other.astype(jnp.float32)


def body(
    resid,
    query_one,
    key_one,
    query_two,
    key_two,
    values,
    mix_lambda,
    segments,
    head_gain,
    out_weight,
    mixer_gain,
    gate_weight,
    up_weight,
    down_weight,
):
    rows = query_one.shape[0]
    heads = mix_lambda.shape[0]
    position = lax.axis_index("sp")
    both_all, down_all = gathered(gate_weight, up_weight, down_weight)
    carried = (key_one, key_two, values, segments)
    earlier = [carried]
    for step in range(REACH):
        carried = shifted((carried[0], carried[1], carried[2], carried[3]), "sp", 1)
        earlier.insert(0, carried)
    width = (REACH + 1) * rows
    k_first = jnp.concatenate([piece[0] for piece in earlier], 0).reshape(width, heads, HD)
    k_second = jnp.concatenate([piece[1] for piece in earlier], 0).reshape(width, heads, HD)
    vals = jnp.concatenate([piece[2] for piece in earlier], 0).reshape(width, heads, VD)
    seg_key = jnp.concatenate([piece[3] for piece in earlier], 0)
    q_pos = position * rows + jnp.arange(rows, dtype=jnp.int32)
    k_pos = (position - REACH) * rows + jnp.arange(width, dtype=jnp.int32)
    allowed = (
        (seg_key[None, :] == segments[:, None])
        & (k_pos[None, :] <= q_pos[:, None])
        & (k_pos[None, :] >= 0)
    )

    def weights(query, keys):
        score = jnp.einsum(
            "qhd,khd->hqk", query.reshape(rows, heads, HD), keys, preferred_element_type=jnp.float32
        ) * HD ** (-0.5)
        score = jnp.where(allowed[None], score, -jnp.inf)
        score = score - jnp.max(score, axis=-1, keepdims=True)
        expo = jnp.exp(score)
        return (expo / jnp.sum(expo, axis=-1, keepdims=True)).astype(jnp.bfloat16)

    out_first = jnp.einsum(
        "hqk,khe->qhe", weights(query_one, k_first), vals, preferred_element_type=jnp.float32
    )
    out_second = jnp.einsum(
        "hqk,khe->qhe", weights(query_two, k_second), vals, preferred_element_type=jnp.float32
    )
    head_out = out_first - mix_lambda[None, :, None] * out_second
    meansq = jnp.mean(head_out * head_out, axis=-1, keepdims=True)
    attn_rows = (
        (head_out * lax.rsqrt(meansq + 1e-05) * head_gain)
        .reshape(rows, heads * VD)
        .astype(jnp.bfloat16)
    )
    projected = jnp.dot(
        whole_channels(attn_rows),
        out_weight,
        preferred_element_type=jnp.float32,
    )
    mid = (resid.astype(jnp.float32) + projected).astype(jnp.bfloat16)
    midf = mid.astype(jnp.float32)
    squares = lax.psum(jnp.sum(midf * midf, axis=1), "tp")
    channels = mid.shape[1] * lax.axis_size("tp")
    normed = (midf * lax.rsqrt(squares / channels + 1e-06)[:, None] * mixer_gain).astype(
        jnp.bfloat16
    )
    members = lax.axis_size("sp")
    paired = len(groups(members)[0][0]) == 2
    if paired:
        normed = jnp.concatenate([normed, swapped(normed, "sp", members)], 0)
    whole_rows = whole_channels(normed)
    whole_rows, both_all, down_all = lax.optimization_barrier((whole_rows, both_all, down_all))
    part = both_all.shape[1] // 2
    gate = jnp.dot(whole_rows, both_all[:, :part], preferred_element_type=jnp.float32)
    up = jnp.dot(whole_rows, both_all[:, part:], preferred_element_type=jnp.float32)
    hidden = (jax.nn.silu(gate) * up).astype(jnp.bfloat16)
    terms = jnp.dot(hidden, down_all, preferred_element_type=jnp.float32)
    summed = own_channels(terms.astype(jnp.bfloat16))
    if paired:
        came = swapped(summed[rows:].astype(jnp.bfloat16), "sp", members)
        summed = summed[:rows] + came.astype(jnp.float32)
    return (midf + summed).astype(jnp.bfloat16)


def solution(mesh):
    in_specs = (
        P("sp", "tp"),
        P("sp", "tp"),
        P("sp", "tp"),
        P("sp", "tp"),
        P("sp", "tp"),
        P("sp", "tp"),
        P("tp"),
        P("sp"),
        P(),
        P(None, "tp"),
        P("tp"),
        P("sp", "tp"),
        P("sp", "tp"),
        P("tp", "sp"),
    )
    out_specs = P("sp", "tp")
    return jax.shard_map(body, mesh=mesh, in_specs=in_specs, out_specs=out_specs, check_vma=False)
```

profile of v0, /device:TPU:16, one launch (start us, length us, event | category | flops | bytes accessed | tf_op | source)
XLA Modules:
  0.0 496.8 jit_solution(3711081791388752364)
XLA Ops:
  10.3 9.3 %collective-permute-done.20 = bf16[1,1536,128]{2,1,0:T(8,128)(2,1)S(1)} collective-permute-done((bf16[1,1536,128]{2,1,0:T(8,128)(2,1)}, bf16[1,1536,128]{2,1,0:T(8,128)(2,1)S(1)}, u32[]{:S(2)}, u32[]{:S(2)}) %collective-permute-start.20) | collective-permute-done | bytes 393248 | tf_op jit(solution)/shard_map/ppermute | solution.py:36
  25.0 16.7 %collective-permute-done.19 = bf16[1,128,3072]{2,1,0:T(8,128)(2,1)} collective-permute-done((bf16[1,128,3072]{2,1,0:T(8,128)(2,1)}, bf16[1,128,3072]{2,1,0:T(8,128)(2,1)}, u32[]{:S(2)}, u32[]{:S(2)}) %collective-permute-start.19) | collective-permute-done | bytes 786464 | tf_op jit(solution)/shard_map/ppermute | solution.py:36
  59.1 9.4 %collective-permute-done.4 = s32[384]{0:T(512)S(1)} collective-permute-done((s32[384]{0:T(512)S(1)}, s32[384]{0:T(512)S(1)}, u32[]{:S(2)}, u32[]{:S(2)}) %collective-permute-start.4) | collective-permute-done | bytes 1568 | tf_op jit(solution)/shard_map/ppermute | solution.py:15
  72.4 53.3 %collective-permute-done.5 = s32[384]{0:T(512)S(1)} collective-permute-done((s32[384]{0:T(512)S(1)}, s32[384]{0:T(512)S(1)}, u32[]{:S(2)}, u32[]{:S(2)}) %collective-permute-start.5) | collective-permute-done | bytes 1568 | tf_op jit(solution)/shard_map/ppermute | solution.py:15
  128.3 22.0 %collective-permute-done.6 = s32[384]{0:T(512)} collective-permute-done((s32[384]{0:T(512)S(1)}, s32[384]{0:T(512)}, u32[]{:S(2)}, u32[]{:S(2)}) %collective-permute-start.6) | collective-permute-done | bytes 1568 | tf_op jit(solution)/shard_map/ppermute | solution.py:15
  152.8 5.1 %collective-permute-done.7 = s32[384]{0:T(512)} collective-permute-done((s32[384]{0:T(512)}, s32[384]{0:T(512)}, u32[]{:S(2)}, u32[]{:S(2)}) %collective-permute-start.7) | collective-permute-done | bytes 1568 | tf_op jit(solution)/shard_map/ppermute | solution.py:15
  164.4 5.7 %collective-permute-start.1 = (bf16[384,1024]{1,0:T(8,128)(2,1)S(1)}, bf16[384,1024]{1,0:T(8,128)(2,1)}, u32[]{:S(2)}, u32[]{:S(2)}) collective-permute-start(bf16[384,1024]{1,0:T(8,128)(2,1)S(1)} %collective-permute-done), channel_id=1, source_target_pairs={{0,2},{2,4},{4,6},{6,8},{8,10},{10,12},{12,14},{14,16},{16,18},{18... | collective-permute-start | bytes 2359304 | tf_op jit(solution)/shard_map/ppermute | solution.py:15
  176.9 18.0 %collective-permute-done.14 = bf16[384,512]{0,1:T(8,128)(2,1)S(1)} collective-permute-done((bf16[384,512]{0,1:T(8,128)(2,1)S(1)}, bf16[384,512]{0,1:T(8,128)(2,1)S(1)}, u32[]{:S(2)}, u32[]{:S(2)}) %collective-permute-start.14) | collective-permute-done | bytes 393248 | tf_op jit(solution)/shard_map/ppermute | solution.py:15
  196.9 3.7 and_and_fusion
  200.6 52.3 %collective-permute-done.10 = bf16[384,512]{0,1:T(8,128)(2,1)S(1)} collective-permute-done((bf16[384,512]{0,1:T(8,128)(2,1)S(1)}, bf16[384,512]{0,1:T(8,128)(2,1)S(1)}, u32[]{:S(2)}, u32[]{:S(2)}) %collective-permute-start.10) | collective-permute-done | bytes 393248 | tf_op jit(solution)/shard_map/ppermute | solution.py:15
  254.8 9.9 %collective-permute-done.15 = bf16[384,512]{0,1:T(8,128)(2,1)S(1)} collective-permute-done((bf16[384,512]{0,1:T(8,128)(2,1)S(1)}, bf16[384,512]{0,1:T(8,128)(2,1)S(1)}, u32[]{:S(2)}, u32[]{:S(2)}) %collective-permute-start.15) | collective-permute-done | bytes 393248 | tf_op jit(solution)/shard_map/ppermute | solution.py:15
  268.3 7.0 %collective-permute-done.11 = bf16[384,512]{0,1:T(8,128)(2,1)S(1)} collective-permute-done((bf16[384,512]{0,1:T(8,128)(2,1)S(1)}, bf16[384,512]{0,1:T(8,128)(2,1)S(1)}, u32[]{:S(2)}, u32[]{:S(2)}) %collective-permute-start.11) | collective-permute-done | bytes 393248 | tf_op jit(solution)/shard_map/ppermute | solution.py:15
  275.5 6.2 %fusion.29 = f32[4,1920,384]{2,1,0:T(8,128)} fusion(bf16[1920,4,128]{0,2,1:T(8,128)(2,1)S(1)} %bitcast.76, bf16[384,512]{1,0:T(8,128)(2,1)S(1)} %copy-done), kind=kOutput, calls=%fused_computation.50 | convolution fusion | flops 754974720 | bytes 14155776 | tf_op jit(solution)/shard_map/qhd,khd->hqk/dot_general | solution.py:121
  281.7 19.0 %fusion.40 = (f32[4,384]{1,0:T(4,128)S(1)}, f32[4,384,1920]{1,2,0:T(8,128)}) fusion(f32[4,1920,384]{2,1,0:T(8,128)} %fusion.29, pred[384,1920]{0,1:T(8,128)(4,1)} %and_and_fusion), kind=kOutput, calls=%fused_computation.96 | output fusion | flops 17696640 | bytes 24336384 | tf_op jit(solution)/shard_map/sub | solution.py:125
  301.8 6.2 %fusion.32 = f32[4,1920,384]{2,1,0:T(8,128)} fusion(bf16[1920,4,128]{0,2,1:T(8,128)(2,1)S(1)} %bitcast.77, bf16[384,512]{1,0:T(8,128)(2,1)S(1)} %copy-done.13), kind=kOutput, calls=%fused_computation.53 | convolution fusion | flops 754974720 | bytes 14155776 | tf_op jit(solution)/shard_map/qhd,khd->hqk/dot_general | solution.py:121
  310.4 17.8 %fusion.41 = (f32[4,384]{1,0:T(4,128)S(1)}, f32[4,384,1920]{1,2,0:T(8,128)}) fusion(f32[4,1920,384]{2,1,0:T(8,128)} %fusion.32, pred[384,1920]{0,1:T(8,128)(4,1)} %and_and_fusion), kind=kOutput, calls=%fused_computation.97 | output fusion | flops 17696640 | bytes 24336384 | tf_op jit(solution)/shard_map/sub | solution.py:125
  328.2 47.6 %collective-permute-done.3 = bf16[384,1024]{1,0:T(8,128)(2,1)S(1)} collective-permute-done((bf16[384,1024]{1,0:T(8,128)(2,1)}, bf16[384,1024]{1,0:T(8,128)(2,1)S(1)}, u32[]{:S(2)}, u32[]{:S(2)}) %collective-permute-start.3) | collective-permute-done | bytes 786464 | tf_op jit(solution)/shard_map/ppermute | solution.py:15
  382.8 6.4 %copy.31 = bf16[1920,1024]{0,1:T(8,128)(2,1)} copy(bf16[1920,1024]{1,0:T(8,128)(2,1)} %constant_dynamic-update-slice_fusion) | data formatting | bytes 7864320 | tf_op jit(solution)/shard_map/concatenate | solution.py:110
  389.2 8.0 %fusion.13 = f32[4,256,384]{2,1,0:T(8,128)S(1)} fusion(bf16[1920,4,256]{0,2,1:T(8,128)(2,1)} %bitcast.69, f32[4,384,1920]{1,2,0:T(8,128)} %get-tuple-element.18, f32[4,384]{1,0:T(4,128)S(1)} %get-tuple-element.17), kind=kOutput, calls=%fused_computation.19 | convolution fusion | flops 1515847680 | bytes 17307648 | tf_op jit(solution)/shard_map/hqk,khe->qhe/dot_general | solution.py:132
  397.2 6.7 %fusion.24 = (f32[384,4]{0,1:T(4,128)S(1)}, f32[4,256,384]{2,1,0:T(8,128)S(1)}) fusion(f32[4,256,384]{2,1,0:T(8,128)S(1)} %fusion.13, f32[4]{0:T(128)S(1)} %copy-done.23, bf16[1920,4,256]{0,2,1:T(8,128)(2,1)S(1)} %bitcast.70, f32[4,384,1920]{1,2,0:T(8,128)} %get-tuple-element.20, f32[4,384]{1,0:T(4,128)S(1)} %get-tuple-element.19), kind=kOutput, calls=%fused_computation.42 | convolution fusion | flops 1517419008 | bytes 18886672 | tf_op jit(solution)/shard_map/hqk,khe->qhe/dot_general | solution.py:129
  411.5 19.6 %collective-permute-done.17 = bf16[384,1024]{1,0:T(8,128)(2,1)S(1)} collective-permute-done((bf16[384,1024]{1,0:T(8,128)(2,1)S(1)}, bf16[384,1024]{1,0:T(8,128)(2,1)S(1)}, u32[]{:S(2)}, u32[]{:S(2)}) %collective-permute-start.17) | collective-permute-done | bytes 786464 | tf_op jit(solution)/shard_map/ppermute | solution.py:57
  435.5 9.6 %fusion.6 = f32[768,1536]{1,0:T(8,128)} fusion(bf16[768,2048]{1,0:T(8,128)(2,1)S(1)} %constant_dynamic-update-slice_fusion.23, bf16[2048,3072]{1,0:T(8,128)(2,1)} %all-gather.3.cloned.1.call-done), kind=kOutput, calls=%fused_computation.12 | convolution fusion | flops 4831838208 | bytes 14155776 | tf_op jit(solution)/shard_map/dot_general | solution.py:161
  445.1 17.8 %convolution_convert_fusion = bf16[768,2048]{1,0:T(8,128)(2,1)} fusion(bf16[1536,2048]{0,1:T(8,128)(2,1)} %all-gather.5.cloned.1.call-done, f32[768,1536]{1,0:T(8,128)} %fusion.6, bf16[768,2048]{1,0:T(8,128)(2,1)S(1)} %constant_dynamic-update-slice_fusion.23, bf16[2048,3072]{1,0:T(8,128)(2,1)} %all-gather.3.cloned.1.call-done), kind=kOutput, calls=%fused_computation.23 | convolution fusion | flops 9672327168 | bytes 23592960 | tf_op jit(solution)/shard_map/dot_general | solution.py:164
  469.2 19.3 %collective-permute-done.22 = bf16[384,1024]{1,0:T(8,128)(2,1)S(1)} collective-permute-done((bf16[384,1024]{1,0:T(8,128)(2,1)S(1)}, bf16[384,1024]{1,0:T(8,128)(2,1)S(1)}, u32[]{:S(2)}, u32[]{:S(2)}) %collective-permute-start.22) | collective-permute-done | bytes 786464 | tf_op jit(solution)/shard_map/ppermute | solution.py:57
  (142 shorter events, 86.1 us)
Async XLA Ops:
  6.5 428.9 %all-gather.5.cloned.1.call-start = ((), (), s32[]{:S(2)}) async-start(), calls=%async_computation.1 | async-start | bytes 7077888 | tf_op jit(solution)/shard_map/all_gather | solution.py:52
  8.5 11.1 %collective-permute-start.20 = (bf16[1,1536,128]{2,1,0:T(8,128)(2,1)}, bf16[1,1536,128]{2,1,0:T(8,128)(2,1)S(1)}, u32[]{:S(2)}, u32[]{:S(2)}) collective-permute-start(bf16[1,1536,128]{2,1,0:T(8,128)(2,1)} %get-tuple-element.15), channel_id=1, source_target_pairs={{0,2},{2,0},{4,6},{6,4},{8,10},{10,8},{12,14},{14,12},{16,18},{18,... | collective-permute-start | bytes 1179656 | tf_op jit(solution)/shard_map/ppermute | solution.py:36
  20.8 414.7 %all-gather.3.cloned.1.call-start = ((), (), s32[]{:S(2)}) async-start(), calls=%async_computation | async-start | bytes 14155776 | tf_op jit(solution)/shard_map/all_gather | solution.py:51
  22.9 18.7 %collective-permute-start.19 = (bf16[1,128,3072]{2,1,0:T(8,128)(2,1)}, bf16[1,128,3072]{2,1,0:T(8,128)(2,1)}, u32[]{:S(2)}, u32[]{:S(2)}) collective-permute-start(bf16[1,128,3072]{2,1,0:T(8,128)(2,1)} %bitcast.10), channel_id=1, source_target_pairs={{0,2},{2,0},{4,6},{6,4},{8,10},{10,8},{12,14},{14,12},{16,18},{18,... | collective-permute-start | bytes 2359304 | tf_op jit(solution)/shard_map/ppermute | solution.py:36
  45.2 25.3 %collective-permute-start.12 = (bf16[384,512]{0,1:T(8,128)(2,1)S(1)}, bf16[384,512]{0,1:T(8,128)(2,1)}, u32[]{:S(2)}, u32[]{:S(2)}) collective-permute-start(bf16[384,512]{0,1:T(8,128)(2,1)S(1)} %copy.37), channel_id=1, source_target_pairs={{0,2},{2,4},{4,6},{6,8},{8,10},{10,12},{12,14},{14,16},{16,18},{18... | collective-permute-start | bytes 1179656 | tf_op jit(solution)/shard_map/ppermute | solution.py:15
  48.6 19.9 %collective-permute-start.4 = (s32[384]{0:T(512)S(1)}, s32[384]{0:T(512)S(1)}, u32[]{:S(2)}, u32[]{:S(2)}) collective-permute-start(s32[384]{0:T(512)S(1)} %copy-done.16), channel_id=1, source_target_pairs={{0,2},{2,4},{4,6},{6,8},{8,10},{10,12},{12,14},{14,16},{16,18},{18... | collective-permute-start | bytes 4616 | tf_op jit(solution)/shard_map/ppermute | solution.py:15
  52.1 112.4 %collective-permute-start = (bf16[384,1024]{1,0:T(8,128)(2,1)S(1)}, bf16[384,1024]{1,0:T(8,128)(2,1)S(1)}, u32[]{:S(2)}, u32[]{:S(2)}) collective-permute-start(bf16[384,1024]{1,0:T(8,128)(2,1)S(1)} %copy-done.10), channel_id=1, source_target_pairs={{0,2},{2,4},{4,6},{6,8},{8,10},{10,12},{12,14},{14,16},{16,18},{18... | collective-permute-start | bytes 2359304 | tf_op jit(solution)/shard_map/ppermute | solution.py:15
  55.7 102.8 %collective-permute-start.8 = (bf16[384,512]{0,1:T(8,128)(2,1)S(1)}, bf16[384,512]{0,1:T(8,128)(2,1)S(1)}, u32[]{:S(2)}, u32[]{:S(2)}) collective-permute-start(bf16[384,512]{0,1:T(8,128)(2,1)S(1)} %copy.32), channel_id=1, source_target_pairs={{0,2},{2,4},{4,6},{6,8},{8,10},{10,12},{12,14},{14,16},{16,18},{18... | collective-permute-start | bytes 1179656 | tf_op jit(solution)/shard_map/ppermute | solution.py:15
  68.6 57.2 %collective-permute-start.5 = (s32[384]{0:T(512)S(1)}, s32[384]{0:T(512)S(1)}, u32[]{:S(2)}, u32[]{:S(2)}) collective-permute-start(s32[384]{0:T(512)S(1)} %collective-permute-done.4), channel_id=1, source_target_pairs={{0,2},{2,4},{4,6},{6,8},{8,10},{10,12},{12,14},{14,16},{16,18},{18... | collective-permute-start | bytes 4616 | tf_op jit(solution)/shard_map/ppermute | solution.py:15
  70.5 89.9 %collective-permute-start.13 = (bf16[384,512]{0,1:T(8,128)(2,1)}, bf16[384,512]{0,1:T(8,128)(2,1)S(1)}, u32[]{:S(2)}, u32[]{:S(2)}) collective-permute-start(bf16[384,512]{0,1:T(8,128)(2,1)} %collective-permute-done.12), channel_id=1, source_target_pairs={{0,2},{2,4},{4,6},{6,8},{8,10},{10,12},{12,14},{14,16},{16,18},{18... | collective-permute-start | bytes 1179656 | tf_op jit(solution)/shard_map/ppermute | solution.py:15
  125.8 24.5 %collective-permute-start.6 = (s32[384]{0:T(512)S(1)}, s32[384]{0:T(512)}, u32[]{:S(2)}, u32[]{:S(2)}) collective-permute-start(s32[384]{0:T(512)S(1)} %collective-permute-done.5), channel_id=1, source_target_pairs={{0,2},{2,4},{4,6},{6,8},{8,10},{10,12},{12,14},{14,16},{16,18},{18... | collective-permute-start | bytes 4616 | tf_op jit(solution)/shard_map/ppermute | solution.py:15
  150.2 7.6 %collective-permute-start.7 = (s32[384]{0:T(512)}, s32[384]{0:T(512)}, u32[]{:S(2)}, u32[]{:S(2)}) collective-permute-start(s32[384]{0:T(512)} %collective-permute-done.6), channel_id=1, source_target_pairs={{0,2},{2,4},{4,6},{6,8},{8,10},{10,12},{12,14},{14,16},{16,18},{18... | collective-permute-start | bytes 4616 | tf_op jit(solution)/shard_map/ppermute | solution.py:15
  158.5 15.7 %collective-permute-start.9 = (bf16[384,512]{0,1:T(8,128)(2,1)S(1)}, bf16[384,512]{0,1:T(8,128)(2,1)S(1)}, u32[]{:S(2)}, u32[]{:S(2)}) collective-permute-start(bf16[384,512]{0,1:T(8,128)(2,1)S(1)} %collective-permute-done.8), channel_id=1, source_target_pairs={{0,2},{2,4},{4,6},{6,8},{8,10},{10,12},{12,14},{14,16},{16,18},{18... | collective-permute-start | bytes 1179656 | tf_op jit(solution)/shard_map/ppermute | solution.py:15
  160.4 34.5 %collective-permute-start.14 = (bf16[384,512]{0,1:T(8,128)(2,1)S(1)}, bf16[384,512]{0,1:T(8,128)(2,1)S(1)}, u32[]{:S(2)}, u32[]{:S(2)}) collective-permute-start(bf16[384,512]{0,1:T(8,128)(2,1)S(1)} %collective-permute-done.13), channel_id=1, source_target_pairs={{0,2},{2,4},{4,6},{6,8},{8,10},{10,12},{12,14},{14,16},{16,18},{18... | collective-permute-start | bytes 1179656 | tf_op jit(solution)/shard_map/ppermute | solution.py:15
  164.4 100.4 %collective-permute-start.1 = (bf16[384,1024]{1,0:T(8,128)(2,1)S(1)}, bf16[384,1024]{1,0:T(8,128)(2,1)}, u32[]{:S(2)}, u32[]{:S(2)}) collective-permute-start(bf16[384,1024]{1,0:T(8,128)(2,1)S(1)} %collective-permute-done), channel_id=1, source_target_pairs={{0,2},{2,4},{4,6},{6,8},{8,10},{10,12},{12,14},{14,16},{16,18},{18... | collective-permute-start | bytes 2359304 | tf_op jit(solution)/shard_map/ppermute | solution.py:15
  174.2 78.7 %collective-permute-start.10 = (bf16[384,512]{0,1:T(8,128)(2,1)S(1)}, bf16[384,512]{0,1:T(8,128)(2,1)S(1)}, u32[]{:S(2)}, u32[]{:S(2)}) collective-permute-start(bf16[384,512]{0,1:T(8,128)(2,1)S(1)} %collective-permute-done.9), channel_id=1, source_target_pairs={{0,2},{2,4},{4,6},{6,8},{8,10},{10,12},{12,14},{14,16},{16,18},{18... | collective-permute-start | bytes 1179656 | tf_op jit(solution)/shard_map/ppermute | solution.py:15
  194.9 69.8 %collective-permute-start.15 = (bf16[384,512]{0,1:T(8,128)(2,1)S(1)}, bf16[384,512]{0,1:T(8,128)(2,1)S(1)}, u32[]{:S(2)}, u32[]{:S(2)}) collective-permute-start(bf16[384,512]{0,1:T(8,128)(2,1)S(1)} %collective-permute-done.14), channel_id=1, source_target_pairs={{0,2},{2,4},{4,6},{6,8},{8,10},{10,12},{12,14},{14,16},{16,18},{18... | collective-permute-start | bytes 1179656 | tf_op jit(solution)/shard_map/ppermute | solution.py:15
  252.9 22.4 %collective-permute-start.11 = (bf16[384,512]{0,1:T(8,128)(2,1)S(1)}, bf16[384,512]{0,1:T(8,128)(2,1)S(1)}, u32[]{:S(2)}, u32[]{:S(2)}) collective-permute-start(bf16[384,512]{0,1:T(8,128)(2,1)S(1)} %collective-permute-done.10), channel_id=1, source_target_pairs={{0,2},{2,4},{4,6},{6,8},{8,10},{10,12},{12,14},{14,16},{16,18},{18... | collective-permute-start | bytes 1179656 | tf_op jit(solution)/shard_map/ppermute | solution.py:15
  264.9 43.1 %collective-permute-start.2 = (bf16[384,1024]{1,0:T(8,128)(2,1)}, bf16[384,1024]{1,0:T(8,128)(2,1)}, u32[]{:S(2)}, u32[]{:S(2)}) collective-permute-start(bf16[384,1024]{1,0:T(8,128)(2,1)} %collective-permute-done.1), channel_id=1, source_target_pairs={{0,2},{2,4},{4,6},{6,8},{8,10},{10,12},{12,14},{14,16},{16,18},{18... | collective-permute-start | bytes 2359304 | tf_op jit(solution)/shard_map/ppermute | solution.py:15
  308.0 67.8 %collective-permute-start.3 = (bf16[384,1024]{1,0:T(8,128)(2,1)}, bf16[384,1024]{1,0:T(8,128)(2,1)S(1)}, u32[]{:S(2)}, u32[]{:S(2)}) collective-permute-start(bf16[384,1024]{1,0:T(8,128)(2,1)} %collective-permute-done.2), channel_id=1, source_target_pairs={{0,2},{2,4},{4,6},{6,8},{8,10},{10,12},{12,14},{14,16},{16,18},{18... | collective-permute-start | bytes 2359304 | tf_op jit(solution)/shard_map/ppermute | solution.py:15
  411.4 19.7 %collective-permute-start.17 = (bf16[384,1024]{1,0:T(8,128)(2,1)S(1)}, bf16[384,1024]{1,0:T(8,128)(2,1)S(1)}, u32[]{:S(2)}, u32[]{:S(2)}) collective-permute-start(bf16[384,1024]{1,0:T(8,128)(2,1)S(1)} %fusion.22), channel_id=1, source_target_pairs={{0,2},{2,0},{4,6},{6,4},{8,10},{10,8},{12,14},{14,12},{16,18},{18,... | collective-permute-start | bytes 2359304 | tf_op jit(solution)/shard_map/ppermute | solution.py:57
  431.8 3.5 collective-permute-start.18
  464.6 3.5 collective-permute-start.21
  468.9 19.6 %collective-permute-start.22 = (bf16[384,1024]{1,0:T(8,128)(2,1)S(1)}, bf16[384,1024]{1,0:T(8,128)(2,1)S(1)}, u32[]{:S(2)}, u32[]{:S(2)}) collective-permute-start(bf16[384,1024]{1,0:T(8,128)(2,1)S(1)} %slice.31), channel_id=1, source_target_pairs={{0,2},{2,0},{4,6},{6,4},{8,10},{10,8},{12,14},{14,12},{16,18},{18,... | collective-permute-start | bytes 2359304 | tf_op jit(solution)/shard_map/ppermute | solution.py:57
  (25 other events, 862.8 us)
Sparse Core Ops, SparseCore 0:
  20.9 125.2 all-gather.4
  148.4 264.6 all-gather.2
where the time goes:
time: 502 us; the launch traced here: 497 us
  waiting for transfers between devices  301 us (60%)
  matrix products  56.3 us (11%)
  starting transfers between devices  45.8 us (9%)
  other arithmetic  44.4 us (9%)
  local copies, waits for them, and re-layouts  32 us (6%)
  between operations  14.3 us (3%)
    ppermute x16, waiting for transfers between devices, shifted(): return lax.ppermute(value, axis, pairs)  228 us
    ppermute x5, waiting for transfers between devices, swapped(): return lax.ppermute(value, axis, [(i, i ^ 1) for i in range(members)])  47.5 us
    ppermute x16, starting transfers between devices, shifted(): return lax.ppermute(value, axis, pairs)  42 us
    sub x2, other arithmetic, weights(): score = score - jnp.max(score, axis=-1, keepdims=True)  36.7 us
    ppermute x2, waiting for transfers between devices, spread(): came = lax.ppermute(sent, 'sp', pairs)  26 us
    dot_general x1, matrix products, body(): terms = jnp.dot(hidden, down_all, preferred_element_type=jnp.float32)  17.8 us
    unnamed x68, local copies, waits for them, and re-layouts  15.6 us
    dot_general x2, matrix products, weights(): jnp.einsum('qhd,khd->hqk', query.reshape(rows, heads, HD), keys, preferre...  12.4 us
  transfers between devices with their start and end apart: 25, of which 17 were waited for; matrix products, arithmetic and copies ran while one was open for 20% of the time, Pallas kernels for 0%

commit v1 on v0

--- a/solution.py
+++ b/solution.py
@@ -1,6 +1,10 @@
+import functools
+
 import jax
 import jax.numpy as jnp
 from jax import lax
+from jax.experimental import pallas as pl
+from jax.experimental.pallas import tpu as pltpu
 from jax.sharding import PartitionSpec as P
 
 HD = 128
@@ -169,6 +173,528 @@
     return (midf + summed).astype(jnp.bfloat16)
 
 
+def rdma(src, dst, send, recv, device):
+    return pltpu.make_async_remote_copy(
+        src_ref=src, dst_ref=dst, send_sem=send, recv_sem=recv,
+        device_id=device, device_id_type=pl.DeviceIdType.MESH,
+    )
+
+
+def layer_kernel(
+    plane, lines, sub,
+    resid, q_one, k_one, q_two, k_two, vals, lam, seg, head_gain, out_w, mix_gain, gate, up, down,
+    out,
+    qb, kb, vb, sb, ao, ar, oww, res, mid, mg, xa, ga, ua, da, hid, pown, psend, precv, csend, crecv,
+    s_qkv, r_qkv, s_halo, r_halo, s_w1, s_w2, r_w, s_ao, r_ao, s_pair, r_pair,
+    s_ag, r_ag, s_xd, r_xd, s_pp, r_pp, s_ch, r_ch, s_loc,
+):
+    sp, tp = lax.axis_index("sp"), lax.axis_index("tp")
+    z, p = lax.div(sp, plane), lax.rem(sp, plane)
+    rows, half = resid.shape
+    heads = plane
+    depth = gate.shape[0]
+    units = gate.shape[1] // lines
+    own_rows = plane * rows
+    px, py = lax.rem(p, 2), lax.div(p, 2)
+
+    def peer(k):
+        a, b = k % 2, k // 2
+        return (py + b - 2 * py * b) * 2 + px + a - 2 * px * a
+
+    def line_peer(d):
+        return lax.rem(z + d, lines)
+
+    partner = (sp, 1 - tp)
+    in_plane = [peer(k) for k in range(1, plane)]
+
+    barrier = pltpu.get_barrier_semaphore()
+    for q in in_plane:
+        pl.semaphore_signal(barrier, inc=1, device_id=(z * plane + q, tp), device_id_type=pl.DeviceIdType.MESH)
+    for d in range(1, lines):
+        pl.semaphore_signal(barrier, inc=1, device_id=(line_peer(d) * plane + p, tp), device_id_type=pl.DeviceIdType.MESH)
+    pl.semaphore_signal(barrier, inc=1, device_id=partner, device_id_type=pl.DeviceIdType.MESH)
+    pl.semaphore_wait(barrier, plane - 1 + lines - 1 + 1)
+
+    sources = (k_one, k_two, vals, q_one, q_two)
+
+    def mul(i, n):
+        return pl.multiple_of(i * n, n)
+
+    def qkv_src(a, head):
+        wide = VD if a == 2 else HD
+        return sources[a].at[:, pl.ds(mul(head, wide), wide)]
+
+    def kv_dst(a, block):
+        at = pl.ds(mul(block, rows), rows)
+        if a == 2:
+            return vb.at[at, :]
+        return kb.at[a, at, :]
+
+    def qkv_dst(a, block):
+        if a == 5:
+            return sb.at[plane + block]
+        if a < 3:
+            return kv_dst(a, plane + block)
+        return qb.at[a - 3, pl.ds(mul(block, rows), rows), :]
+
+    def qkv_copy(k, a):
+        q = in_plane[k]
+        src = seg if a == 5 else qkv_src(a, q)
+        return rdma(src, qkv_dst(a, p), s_qkv.at[k, a], r_qkv.at[p, a], (z * plane + q, tp))
+
+    def halo_copy(block, a, own):
+        if a == 3:
+            src = seg if own else sb.at[plane + block]
+            dst = sb.at[block]
+        else:
+            src = qkv_src(a, p) if own else kv_dst(a, plane + block)
+            dst = kv_dst(a, block)
+        return rdma(src, dst, s_halo.at[block, a], r_halo.at[block, a], (sp + plane, tp))
+
+    def weight_dst(s, a):
+        if a == 0:
+            return ga.at[pl.ds(mul(s, depth), depth), :]
+        if a == 1:
+            return ua.at[pl.ds(mul(s, depth), depth), :]
+        return da.at[:, pl.ds(mul(s, depth), depth)]
+
+    def weight_src(line, a):
+        at = pl.ds(mul(line, units), units)
+        if a == 0:
+            return gate.at[:, at]
+        if a == 1:
+            return up.at[:, at]
+        return down.at[at, :]
+
+    def w1_copy(d, a):
+        zz = line_peer(d)
+        return rdma(weight_src(zz, a), weight_dst(sp, a), s_w1.at[d - 1, a], r_w.at[sp, a], (zz * plane + p, tp))
+
+    def w2_copy(k, d, a):
+        s = line_peer(d) * plane + p
+        src = weight_src(z, a) if d == 0 else weight_dst(s, a)
+        return rdma(src, weight_dst(s, a), s_w2.at[k, d, a], r_w.at[s, a], (z * plane + in_plane[k], tp))
+
+    def arrived(dst, sem):
+        rdma(dst, dst, s_pair.at[0], sem, partner).wait_recv()
+
+    def local(src, dst, i):
+        return pltpu.make_async_copy(src, dst, s_loc.at[i])
+
+    for a in (0, 1, 2, 5):
+        for k in range(plane - 1):
+            qkv_copy(k, a).start()
+    for k in range(plane - 1):
+        for a in (3, 4):
+            qkv_copy(k, a).start()
+
+    @pl.when(z < lines - 1)
+    def _():
+        for a in range(4):
+            halo_copy(p, a, True).start()
+
+    for d in range(1, lines):
+        w1_copy(d, 0).start()
+
+    locals_ = [local(qkv_src(a, p), qkv_dst(a, p), a) for a in range(5)]
+    locals_.append(local(out_w, oww, 5))
+    locals_.append(local(resid, res, 6))
+    for a in range(3):
+        locals_.append(local(weight_src(z, a), weight_dst(sp, a), 7 + a))
+    for c in locals_:
+        c.start()
+    sb[plane + p] = seg[...]
+    mg[tp] = mix_gain[...]
+    rdma(mix_gain, mg.at[tp], s_pair.at[0], r_pair.at[0], partner).start()
+
+    for a in range(3):
+        for k in range(plane - 1):
+            w2_copy(k, 0, a).start()
+
+    @pl.when(z == 0)
+    def _():
+        vb[: plane * rows, :] = jnp.zeros((plane * rows, VD), vb.dtype)
+        kb[:, : plane * rows, :] = jnp.zeros((2, plane * rows, HD), kb.dtype)
+        for b in range(plane):
+            sb[b] = jnp.full(sb.shape[1:], -1, sb.dtype)
+
+    for k in range(plane - 1):
+        q = in_plane[k]
+        for a in (0, 1, 2, 5):
+            arrived(qkv_dst(a, q), r_qkv.at[q, a])
+
+        @pl.when(z < lines - 1)
+        def _():
+            for a in range(4):
+                halo_copy(q, a, False).start()
+
+    for d in range(1, lines):
+        for a in (1, 2):
+            w1_copy(d, a).start()
+    for k in range(plane - 1):
+        q = in_plane[k]
+        for a in (3, 4):
+            arrived(qkv_dst(a, q), r_qkv.at[q, a])
+    for c in locals_[:5]:
+        c.wait()
+
+    def forward_weights(a):
+        for d in range(1, lines):
+            s = line_peer(d) * plane + p
+            arrived(weight_dst(s, a), r_w.at[s, a])
+            for k in range(plane - 1):
+                w2_copy(k, d, a).start()
+
+    forward_weights(0)
+
+    scale = HD ** (-0.5) * 1.4426950408889634
+    window = (REACH + 1) * rows
+
+    def ao_remote(j):
+        at = pl.ds(mul(tp * heads + p, VD), VD)
+        return rdma(ao.at[j], ar.at[:, at], s_ao.at[j], r_ao.at[p], (z * plane + j, tp))
+
+    def ao_local(j):
+        at = pl.ds(mul(tp * heads + p, VD), VD)
+        return local(ao.at[j], ar.at[:, at], 10)
+
+    coef = lam[p]
+
+    def query_block(i, carry):
+        j = plane - 1 - i
+
+        @pl.when(z > 0)
+        def _():
+            for a in range(3):
+                arrived(kv_dst(a, j), r_halo.at[j, a])
+            arrived(sb.at[j], r_halo.at[j, 3])
+
+        at = pl.ds(mul(j, rows), window)
+        key_seg = jnp.concatenate([sb[j + n] for n in range(REACH + 1)], axis=1).astype(jnp.float32)
+        own_seg = jnp.broadcast_to(sb[plane + j].astype(jnp.float32), (128, rows))
+        seg_col = jnp.transpose(own_seg)[:, :1]
+        for u in range(rows // sub):
+            col = lax.broadcasted_iota(jnp.int32, (sub, window), 1)
+            row = lax.broadcasted_iota(jnp.int32, (sub, window), 0) + (REACH * rows + u * sub)
+            ok = (key_seg == seg_col[u * sub : (u + 1) * sub]) & (col <= row)
+            outs = []
+            for m in range(2):
+                q = qb[m, pl.ds(pl.multiple_of(j * rows + u * sub, sub), sub), :]
+                s = lax.dot_general(
+                    q, kb[m, at, :], (((1,), (1,)), ((), ())), preferred_element_type=jnp.float32
+                )
+                s = jnp.where(ok, s, -1e30)
+                top = jnp.max(s, axis=1, keepdims=True)
+                e = jnp.exp2((s - top) * scale)
+                total = jnp.sum(e, axis=1, keepdims=True)
+                o = jnp.dot(e.astype(jnp.bfloat16), vb[at, :], preferred_element_type=jnp.float32)
+                outs.append(o / total)
+            h = outs[0] - coef * outs[1]
+            ms = jnp.mean(h * h, axis=1, keepdims=True)
+            h = h * lax.rsqrt(ms + 1e-05) * head_gain[...]
+            ao[j, pl.ds(u * sub, sub), :] = h.astype(ao.dtype)
+
+        @pl.when(j != p)
+        def _():
+            ao_remote(j).start()
+
+        @pl.when(j == p)
+        def _():
+            ao_local(j).start()
+
+        return carry
+
+    lax.fori_loop(0, plane, query_block, 0)
+
+    ao_local(p).wait()
+    for q in in_plane:
+        at = pl.ds(mul(tp * heads + q, VD), VD)
+        arrived(ar.at[:, at], r_ao.at[q])
+    mine = pl.ds(mul(tp, half), half)
+    theirs = pl.ds(mul(1 - tp, half), half)
+    swap = rdma(ar.at[:, mine], ar.at[:, mine], s_pair.at[1], r_pair.at[1], partner)
+    swap.start()
+    for c in locals_[5:7]:
+        c.wait()
+    acc = jnp.dot(ar[:, mine], oww[mine, :], preferred_element_type=jnp.float32)
+    arrived(ar.at[:, theirs], r_pair.at[1])
+    acc = acc + jnp.dot(ar[:, theirs], oww[theirs, :], preferred_element_type=jnp.float32)
+    mid[tp] = (res[...].astype(jnp.float32) + acc).astype(mid.dtype)
+    swap_mid = rdma(mid.at[tp], mid.at[tp], s_pair.at[2], r_pair.at[2], partner)
+    swap_mid.start()
+    arrived(mid.at[1 - tp], r_pair.at[2])
+    arrived(mg.at[1 - tp], r_pair.at[0])
+    m0, m1 = mid[0].astype(jnp.float32), mid[1].astype(jnp.float32)
+    squares = jnp.sum(m0 * m0, axis=1, keepdims=True) + jnp.sum(m1 * m1, axis=1, keepdims=True)
+    inv = lax.rsqrt(squares / (2 * half) + 1e-06)
+    xa[z, 0] = (m0 * inv * mg[0]).astype(xa.dtype)
+    xa[z, 1] = (m1 * inv * mg[1]).astype(xa.dtype)
+
+    def ag_copy(b, to):
+        return rdma(xa.at[b, tp], xa.at[b, tp], s_ag.at[b, to], r_ag.at[b], (sp + plane * (2 * to - 1), tp))
+
+    def xd_copy(b):
+        return rdma(xa.at[b, tp], xa.at[b, tp], s_xd.at[b], r_xd.at[b], partner)
+
+    @pl.when(z < lines - 1)
+    def _():
+        ag_copy(z, 1).start()
+
+    @pl.when(z > 0)
+    def _():
+        ag_copy(z, 0).start()
+
+    def gather_step(d):
+        below, above = z - d, z + d
+
+        @pl.when(below >= 0)
+        def _():
+            arrived(xa.at[below, tp], r_ag.at[below])
+
+            @pl.when(z < lines - 1)
+            def _():
+                ag_copy(below, 1).start()
+
+            xd_copy(below).start()
+
+        @pl.when(above < lines)
+        def _():
+            arrived(xa.at[above, tp], r_ag.at[above])
+
+            @pl.when(z > 0)
+            def _():
+                ag_copy(above, 0).start()
+
+            xd_copy(above).start()
+
+    forward_weights(1)
+    gather_step(1)
+    forward_weights(2)
+    for d in range(2, lines):
+        gather_step(d)
+
+    for c in locals_[7:]:
+        c.wait()
+    for k in range(plane - 1):
+        for d in range(lines):
+            s = line_peer(d) * plane + in_plane[k]
+            for a in range(3):
+                arrived(weight_dst(s, a), r_w.at[s, a])
+
+    low = 2 * z < lines
+
+    def order(i):
+        down_first = jnp.where(i < lines - 1 - z, lines - 1 - i, i - (lines - 1 - z))
+        up_first = jnp.where(i < z, i, lines - 1 - (i - z))
+        b = jnp.where(low, down_first, up_first)
+        return jnp.where(i == lines - 1, z, b)
+
+    tile = units // 3
+
+    def mixer(i):
+        b = order(i)
+
+        @pl.when(b != z)
+        def _():
+            arrived(xa.at[b, 1 - tp], r_xd.at[b])
+
+        def hidden_tile(u, carry):
+            at = pl.ds(mul(u, tile), tile)
+            g = jnp.dot(xa[b, 0], ga[:half, at], preferred_element_type=jnp.float32)
+            g = g + jnp.dot(xa[b, 1], ga[half:, at], preferred_element_type=jnp.float32)
+            v = jnp.dot(xa[b, 0], ua[:half, at], preferred_element_type=jnp.float32)
+            v = v + jnp.dot(xa[b, 1], ua[half:, at], preferred_element_type=jnp.float32)
+            hid[:, at] = (g / (1.0 + jnp.exp(-g)) * v).astype(hid.dtype)
+            return carry
+
+        lax.fori_loop(0, units // tile, hidden_tile, 0)
+        wide = half // 2
+
+        def down_tile(c, carry):
+            theirs_at = pl.ds(pl.multiple_of((1 - tp) * half + c * wide, wide), wide)
+            own_at = pl.ds(pl.multiple_of(tp * half + c * wide, wide), wide)
+            at = pl.ds(mul(c, wide), wide)
+            o = jnp.dot(hid[...], da[:, theirs_at], preferred_element_type=jnp.float32)
+            psend[b, :, at] = o.astype(psend.dtype)
+            o = jnp.dot(hid[...], da[:, own_at], preferred_element_type=jnp.float32)
+            pown[b, :, at] = o
+            return carry
+
+        lax.fori_loop(0, half // wide, down_tile, 0)
+        rdma(psend.at[b], precv.at[b], s_pp.at[b], r_pp.at[b], partner).start()
+
+    def chain_copy(b, to):
+        near = jnp.where(b == z + 1, lines, b) if to == 1 else b
+        return rdma(csend.at[b], crecv.at[near], s_ch.at[b], r_ch.at[near], (sp + plane * (2 * to - 1), tp))
+
+    def chain(i):
+        b = order(i)
+        arrived(precv.at[b], r_pp.at[b])
+        incoming = ((b < z) & (z < lines - 1)) | ((b > z) & (z > 0))
+
+        @pl.when(incoming)
+        def _():
+            arrived(crecv.at[b], r_ch.at[b])
+            csend[b] = (pown[b] + precv[b].astype(jnp.float32) + crecv[b].astype(jnp.float32)).astype(csend.dtype)
+
+        @pl.when(jnp.logical_not(incoming))
+        def _():
+            csend[b] = (pown[b] + precv[b].astype(jnp.float32)).astype(csend.dtype)
+
+        @pl.when(b > z)
+        def _():
+            chain_copy(b, 1).start()
+
+        @pl.when(b < z)
+        def _():
+            chain_copy(b, 0).start()
+
+    def mixer_step(i, carry):
+        mixer(i)
+
+        @pl.when(i > 0)
+        def _():
+            chain(i - 1)
+
+        return carry
+
+    lax.fori_loop(0, lines, mixer_step, 0)
+    arrived(precv.at[z], r_pp.at[z])
+    pown[z] = pown[z] + precv[z].astype(jnp.float32) + mid[tp].astype(jnp.float32)
+
+    @pl.when(z < lines - 1)
+    def _():
+        arrived(crecv.at[z], r_ch.at[z])
+        pown[z] = pown[z] + crecv[z].astype(jnp.float32)
+
+    @pl.when(z > 0)
+    def _():
+        arrived(crecv.at[lines], r_ch.at[lines])
+        pown[z] = pown[z] + crecv[lines].astype(jnp.float32)
+
+    out[...] = pown[z].astype(out.dtype)
+
+    for k in range(plane - 1):
+        for a in range(6):
+            qkv_copy(k, a).wait_send()
+        for d in range(lines):
+            for a in range(3):
+                w2_copy(k, d, a).wait_send()
+    for d in range(1, lines):
+        for a in range(3):
+            w1_copy(d, a).wait_send()
+
+    @pl.when(z < lines - 1)
+    def _():
+        for a in range(4):
+            halo_copy(p, a, True).wait_send()
+            for q in in_plane:
+                halo_copy(q, a, False).wait_send()
+
+    for q in in_plane:
+        ao_remote(q).wait_send()
+    rdma(mix_gain, mg.at[tp], s_pair.at[0], r_pair.at[0], partner).wait_send()
+    swap.wait_send()
+    swap_mid.wait_send()
+    for b in range(lines):
+        rdma(psend.at[b], precv.at[b], s_pp.at[b], r_pp.at[b], partner).wait_send()
+
+        @pl.when(b != z)
+        def _():
+            xd_copy(b).wait_send()
+
+        @pl.when((b <= z) & (z < lines - 1))
+        def _():
+            ag_copy(b, 1).wait_send()
+
+        @pl.when((b >= z) & (z > 0))
+        def _():
+            ag_copy(b, 0).wait_send()
+
+        @pl.when(b > z)
+        def _():
+            chain_copy(b, 1).wait_send()
+
+        @pl.when(b < z)
+        def _():
+            chain_copy(b, 0).wait_send()
+
+
+def fast_body(resid, query_one, key_one, query_two, key_two, values, mix_lambda, segments, head_gain,
+              out_weight, mixer_gain, gate_weight, up_weight, down_weight):
+    plane = mix_lambda.shape[0]
+    lines = lax.axis_size("sp") // plane
+    rows, half = resid.shape
+    depth, units = gate_weight.shape[0], gate_weight.shape[1] // lines
+    full = depth * plane * lines
+    bf, f32 = jnp.bfloat16, jnp.float32
+    sub = rows // 3
+    dma = pltpu.SemaphoreType.DMA
+    anywhere = pl.BlockSpec(memory_space=pl.ANY)
+    vmem = pl.BlockSpec(memory_space=pltpu.VMEM)
+    smem = pl.BlockSpec(memory_space=pltpu.SMEM)
+    flops = 6 * rows * plane * full * units + 2 * rows * full * half + 24 * rows * plane * rows * 5 * VD
+    return pl.pallas_call(
+        functools.partial(layer_kernel, plane, lines, sub),
+        out_shape=jax.ShapeDtypeStruct((rows, half), bf),
+        in_specs=[anywhere] * 6 + [smem, vmem, vmem, anywhere, vmem, anywhere, anywhere, anywhere],
+        out_specs=vmem,
+        scratch_shapes=[
+            pltpu.VMEM((2, plane * rows, HD), bf),
+            pltpu.VMEM((2, 2 * plane * rows, HD), bf),
+            pltpu.VMEM((2 * plane * rows, VD), bf),
+            pltpu.VMEM((2 * plane, 1, rows), jnp.int32),
+            pltpu.VMEM((plane, rows, VD), bf),
+            pltpu.VMEM((rows, full), bf),
+            pltpu.VMEM((full, half), bf),
+            pltpu.VMEM((rows, half), bf),
+            pltpu.VMEM((2, rows, half), bf),
+            pltpu.VMEM((2, 1, half), f32),
+            pltpu.VMEM((lines, 2, rows, half), bf),
+            pltpu.VMEM((full, units), bf),
+            pltpu.VMEM((full, units), bf),
+            pltpu.VMEM((units, full), bf),
+            pltpu.VMEM((rows, units), bf),
+            pltpu.VMEM((lines, rows, half), f32),
+            pltpu.VMEM((lines, rows, half), bf),
+            pltpu.VMEM((lines, rows, half), bf),
+            pltpu.VMEM((lines, rows, half), bf),
+            pltpu.VMEM((lines + 1, rows, half), bf),
+            dma((plane - 1, 6)), dma((plane, 6)),
+            dma((plane, 4)), dma((plane, 4)),
+            dma((lines - 1, 3)), dma((plane - 1, lines, 3)), dma((plane * lines, 3)),
+            dma((plane,)), dma((plane,)),
+            dma((3,)), dma((3,)),
+            dma((lines, 2)), dma((lines,)),
+            dma((lines,)), dma((lines,)),
+            dma((lines,)), dma((lines,)),
+            dma((lines,)), dma((lines + 1,)),
+            dma((11,)),
+        ],
+        compiler_params=pltpu.CompilerParams(
+            collective_id=0, has_side_effects=True, vmem_limit_bytes=60 * 1024 * 1024
+        ),
+        cost_estimate=pl.CostEstimate(flops=flops, bytes_accessed=2 * full * units, transcendentals=0),
+        name="layer",
+    )(resid, query_one, key_one, query_two, key_two, values, mix_lambda, segments.reshape(1, rows),
+      head_gain.reshape(1, VD), out_weight, mixer_gain.reshape(1, half), gate_weight, up_weight, down_weight)
+
+
+def fits(mesh):
+    sp, tp = mesh.shape["sp"], mesh.shape["tp"]
+    return tp == 2 and sp % (REACH * 2) == 0
+
+
+def choose(mesh):
+    def step(*args):
+        heads = args[6].shape[0]
+        if fits(mesh) and heads == REACH:
+            return fast_body(*args)
+        return body(*args)
+
+    return step
+
+
 def solution(mesh):
     in_specs = (
         P("sp", "tp"),
@@ -187,4 +713,4 @@
         P("tp", "sp"),
     )
     out_specs = P("sp", "tp")
-    return jax.shard_map(body, mesh=mesh, in_specs=in_specs, out_specs=out_specs, check_vma=False)
+    return jax.shard_map(choose(mesh), mesh=mesh, in_specs=in_specs, out_specs=out_specs, check_vma=False)

time: 502 us -> 227 us (0.45)
  the two profiles are of different devices: /device:TPU:16 before, /device:TPU:0 now
where the time goes in v1:
time: 227 us; the launch traced here: 225 us
  Pallas kernels  221 us (97%)
  local copies, waits for them, and re-layouts  3.31 us (1%)
    pallas_call x1, Pallas kernels, fast_body(): pl.pallas_call(functools.partial(layer_kernel, plane, lines, sub), out_sh...  221 us

profile of v1, /device:TPU:0, one launch (start us, length us, event | category | flops | bytes accessed | tf_op | source)
XLA Modules:
  0.0 224.7 jit_solution(15077878429918679785)
XLA Ops:
  0.0 1.2 reshape.9.seg
  1.2 221.4 %layer.1 = bf16[384,1024]{1,0:T(8,128)(2,1)} custom-call(bf16[384,1024]{1,0:T(8,128)(2,1)} %resid.1, bf16[384,512]{1,0:T(8,128)(2,1)} %q_one.1, bf16[384,512]{1,0:T(8,128)(2,1)} %k_one.1, bf16[384,512]{1,0:T(8,128)(2,1)} %q_two.1, bf16[384,512]{1,0:T(8,128)(2,1)} %k_two.1, bf16[384,1024]{1,0:T(8,128)(2,1)} %vals.1, f32[4]{0:T(128)} %lam.1, ...), custom_call_target="tpu_custom_call" | custom-call | flops 34225520640 | bytes 3145728 | tf_op jit(solution)/shard_map/layer/pallas_call | solution.py:637
  222.6 2.1 copy.16

commit v2 on v1

--- a/solution.py
+++ b/solution.py
@@ -181,11 +181,11 @@
 
 
 def layer_kernel(
-    plane, lines, sub,
+    plane, lines, sub, pieces,
     resid, q_one, k_one, q_two, k_two, vals, lam, seg, head_gain, out_w, mix_gain, gate, up, down,
     out,
     qb, kb, vb, sb, ao, ar, oww, res, mid, mg, xa, ga, ua, da, hid, pown, psend, precv, csend, crecv,
-    s_qkv, r_qkv, s_halo, r_halo, s_w1, s_w2, r_w, s_ao, r_ao, s_pair, r_pair,
+    s_qkv, r_qkv, s_halo, r_halo, s_w1, s_w2, s_relay, r_w, s_ao, r_ao, s_pair, r_pair,
     s_ag, r_ag, s_xd, r_xd, s_pp, r_pp, s_ch, r_ch, s_loc,
 ):
     sp, tp = lax.axis_index("sp"), lax.axis_index("tp")
@@ -273,7 +273,31 @@
     def w2_copy(k, d, a):
         s = line_peer(d) * plane + p
         src = weight_src(z, a) if d == 0 else weight_dst(s, a)
-        return rdma(src, weight_dst(s, a), s_w2.at[k, d, a], r_w.at[s, a], (z * plane + in_plane[k], tp))
+        return rdma(src, weight_dst(s, a), s_w2.at[k - 1, d, a], r_w.at[s, a], (z * plane + peer(k), tp))
+
+    def relay_copy(d, a):
+        k = 1 + (d + a) % 2
+        s = line_peer(d) * plane + peer(k)
+        return rdma(weight_dst(s, a), weight_dst(s, a), s_relay.at[d, a], r_w.at[s, a], (z * plane + peer(3 - k), tp))
+
+    def weight_arrived(d, a, q):
+        s = line_peer(d) * plane + q
+        arrived(weight_dst(s, a), r_w.at[s, a])
+
+    def spread(d, a):
+        if d > 0:
+            weight_arrived(d, a, p)
+        for k in (1, 2):
+            w2_copy(k, d, a).start()
+
+    def relay(d, a):
+        weight_arrived(d, a, peer(1 + (d + a) % 2))
+        relay_copy(d, a).start()
+
+    def rest_of_weights(a):
+        for d in range(lines):
+            weight_arrived(d, a, peer(2 - (d + a) % 2))
+            weight_arrived(d, a, peer(3))
 
     def arrived(dst, sem):
         rdma(dst, dst, s_pair.at[0], sem, partner).wait_recv()
@@ -293,8 +317,12 @@
         for a in range(4):
             halo_copy(p, a, True).start()
 
-    for d in range(1, lines):
-        w1_copy(d, 0).start()
+    for a in range(3):
+        for d in range(1, lines):
+
+            @pl.when(line_peer(d) < z)
+            def _():
+                w1_copy(d, a).start()
 
     locals_ = [local(qkv_src(a, p), qkv_dst(a, p), a) for a in range(5)]
     locals_.append(local(out_w, oww, 5))
@@ -307,9 +335,8 @@
     mg[tp] = mix_gain[...]
     rdma(mix_gain, mg.at[tp], s_pair.at[0], r_pair.at[0], partner).start()
 
-    for a in range(3):
-        for k in range(plane - 1):
-            w2_copy(k, 0, a).start()
+    for a in range(2):
+        spread(0, a)
 
     @pl.when(z == 0)
     def _():
@@ -318,8 +345,9 @@
         for b in range(plane):
             sb[b] = jnp.full(sb.shape[1:], -1, sb.dtype)
 
-    for k in range(plane - 1):
-        q = in_plane[k]
+    nearest = jnp.maximum(peer(1), peer(2))
+    other = jnp.minimum(peer(1), peer(2))
+    for q in (nearest, jnp.maximum(other, peer(3)), jnp.minimum(other, peer(3))):
         for a in (0, 1, 2, 5):
             arrived(qkv_dst(a, q), r_qkv.at[q, a])
 
@@ -328,9 +356,6 @@
             for a in range(4):
                 halo_copy(q, a, False).start()
 
-    for d in range(1, lines):
-        for a in (1, 2):
-            w1_copy(d, a).start()
     for k in range(plane - 1):
         q = in_plane[k]
         for a in (3, 4):
@@ -338,15 +363,6 @@
     for c in locals_[:5]:
         c.wait()
 
-    def forward_weights(a):
-        for d in range(1, lines):
-            s = line_peer(d) * plane + p
-            arrived(weight_dst(s, a), r_w.at[s, a])
-            for k in range(plane - 1):
-                w2_copy(k, d, a).start()
-
-    forward_weights(0)
-
     scale = HD ** (-0.5) * 1.4426950408889634
     window = (REACH + 1) * rows
 
@@ -368,6 +384,13 @@
             for a in range(3):
                 arrived(kv_dst(a, j), r_halo.at[j, a])
             arrived(sb.at[j], r_halo.at[j, 3])
+
+        for a in range(3):
+            for d in range(1, lines):
+
+                @pl.when((i == plane - 1) & (line_peer(d) > z))
+                def _():
+                    w1_copy(d, a).start()
 
         at = pl.ds(mul(j, rows), window)
         key_seg = jnp.concatenate([sb[j + n] for n in range(REACH + 1)], axis=1).astype(jnp.float32)
@@ -405,6 +428,9 @@
         return carry
 
     lax.fori_loop(0, plane, query_block, 0)
+    spread(0, 2)
+    relay(0, 0)
+    relay(0, 1)
 
     ao_local(p).wait()
     for q in in_plane:
@@ -430,70 +456,56 @@
     xa[z, 0] = (m0 * inv * mg[0]).astype(xa.dtype)
     xa[z, 1] = (m1 * inv * mg[1]).astype(xa.dtype)
 
-    def ag_copy(b, to):
-        return rdma(xa.at[b, tp], xa.at[b, tp], s_ag.at[b, to], r_ag.at[b], (sp + plane * (2 * to - 1), tp))
+    piece = rows // pieces
+
+    def ag_copy(b, to, c):
+        ref = xa.at[b, tp, pl.ds(c * piece, piece), :]
+        return rdma(ref, ref, s_ag.at[b, to, c], r_ag.at[b, c], (sp + plane * (2 * to - 1), tp))
 
     def xd_copy(b):
         return rdma(xa.at[b, tp], xa.at[b, tp], s_xd.at[b], r_xd.at[b], partner)
 
-    @pl.when(z < lines - 1)
-    def _():
-        ag_copy(z, 1).start()
-
-    @pl.when(z > 0)
-    def _():
-        ag_copy(z, 0).start()
-
-    def gather_step(d):
-        below, above = z - d, z + d
+    for c in range(pieces):
+
+        @pl.when(z < lines - 1)
+        def _():
+            ag_copy(z, 1, c).start()
+
+        @pl.when(z > 0)
+        def _():
+            ag_copy(z, 0, c).start()
+
+    def from_above(d):
+        above = z + d
+
+        @pl.when(above < lines)
+        def _():
+            for c in range(pieces):
+                arrived(xa.at[above, tp, pl.ds(c * piece, piece), :], r_ag.at[above, c])
+
+                @pl.when(z > 0)
+                def _():
+                    ag_copy(above, 0, c).start()
+
+            xd_copy(above).start()
+
+    def from_below(d):
+        below = z - d
 
         @pl.when(below >= 0)
         def _():
-            arrived(xa.at[below, tp], r_ag.at[below])
-
-            @pl.when(z < lines - 1)
-            def _():
-                ag_copy(below, 1).start()
+            for c in range(pieces):
+                arrived(xa.at[below, tp, pl.ds(c * piece, piece), :], r_ag.at[below, c])
+
+                @pl.when(z < lines - 1)
+                def _():
+                    ag_copy(below, 1, c).start()
 
             xd_copy(below).start()
 
-        @pl.when(above < lines)
-        def _():
-            arrived(xa.at[above, tp], r_ag.at[above])
-
-            @pl.when(z > 0)
-            def _():
-                ag_copy(above, 0).start()
-
-            xd_copy(above).start()
-
-    forward_weights(1)
-    gather_step(1)
-    forward_weights(2)
-    for d in range(2, lines):
-        gather_step(d)
-
-    for c in locals_[7:]:
-        c.wait()
-    for k in range(plane - 1):
-        for d in range(lines):
-            s = line_peer(d) * plane + in_plane[k]
-            for a in range(3):
-                arrived(weight_dst(s, a), r_w.at[s, a])
-
-    low = 2 * z < lines
-
-    def order(i):
-        down_first = jnp.where(i < lines - 1 - z, lines - 1 - i, i - (lines - 1 - z))
-        up_first = jnp.where(i < z, i, lines - 1 - (i - z))
-        b = jnp.where(low, down_first, up_first)
-        return jnp.where(i == lines - 1, z, b)
-
     tile = units // 3
 
-    def mixer(i):
-        b = order(i)
-
+    def hidden_block(b):
         @pl.when(b != z)
         def _():
             arrived(xa.at[b, 1 - tp], r_xd.at[b])
@@ -504,82 +516,157 @@
             g = g + jnp.dot(xa[b, 1], ga[half:, at], preferred_element_type=jnp.float32)
             v = jnp.dot(xa[b, 0], ua[:half, at], preferred_element_type=jnp.float32)
             v = v + jnp.dot(xa[b, 1], ua[half:, at], preferred_element_type=jnp.float32)
-            hid[:, at] = (g / (1.0 + jnp.exp(-g)) * v).astype(hid.dtype)
+            hid[b, :, at] = (g / (1.0 + jnp.exp(-g)) * v).astype(hid.dtype)
             return carry
 
         lax.fori_loop(0, units // tile, hidden_tile, 0)
-        wide = half // 2
-
+
+    def next_block(i):
+        upper = lines - 1 - z
+        return jnp.where(i < upper, z + 1 + i, z - 1 - (i - upper))
+
+    for d in range(1, lines):
+        spread(d, 0)
+    relay(0, 2)
+    for d in range(1, lines):
+        spread(d, 1)
+    for d in range(1, lines):
+        relay(d, 0)
+    from_above(1)
+    for d in range(1, lines):
+        relay(d, 1)
+        spread(d, 2)
+    from_above(2)
+    from_below(1)
+    for c in locals_[7:]:
+        c.wait()
+    rest_of_weights(0)
+    rest_of_weights(1)
+    hidden_block(z)
+    for d in range(1, lines):
+        relay(d, 2)
+    hidden_block(next_block(0))
+    from_below(2)
+
+    def rank(zz):
+        far = list(range(2, lines)) + [1]
+        back = [lines - 1 - b for b in far]
+        travel = [
+            (far.index(b) + zz if b > zz else back.index(b) + lines - 1 - zz, b) for b in range(lines) if b != zz
+        ]
+        return [b for _, b in sorted(travel)] + [zz]
+
+    def order(i):
+        b = rank(0)[i]
+        for zz in range(1, lines):
+            b = jnp.where(z == zz, rank(zz)[i], b)
+        return b
+
+    wide = half // 2
+
+    def down_block(b):
         def down_tile(c, carry):
             theirs_at = pl.ds(pl.multiple_of((1 - tp) * half + c * wide, wide), wide)
             own_at = pl.ds(pl.multiple_of(tp * half + c * wide, wide), wide)
             at = pl.ds(mul(c, wide), wide)
-            o = jnp.dot(hid[...], da[:, theirs_at], preferred_element_type=jnp.float32)
+            o = jnp.dot(hid[b], da[:, theirs_at], preferred_element_type=jnp.float32)
             psend[b, :, at] = o.astype(psend.dtype)
-            o = jnp.dot(hid[...], da[:, own_at], preferred_element_type=jnp.float32)
+            o = jnp.dot(hid[b], da[:, own_at], preferred_element_type=jnp.float32)
             pown[b, :, at] = o
             return carry
 
         lax.fori_loop(0, half // wide, down_tile, 0)
         rdma(psend.at[b], precv.at[b], s_pp.at[b], r_pp.at[b], partner).start()
 
-    def chain_copy(b, to):
+    def chain_copy(b, to, c):
         near = jnp.where(b == z + 1, lines, b) if to == 1 else b
-        return rdma(csend.at[b], crecv.at[near], s_ch.at[b], r_ch.at[near], (sp + plane * (2 * to - 1), tp))
-
-    def chain(i):
-        b = order(i)
+        at = pl.ds(c * piece, piece)
+        return rdma(
+            csend.at[b, at, :], crecv.at[near, at, :], s_ch.at[b, c], r_ch.at[near, c],
+            (sp + plane * (2 * to - 1), tp),
+        )
+
+    def chain(b):
         arrived(precv.at[b], r_pp.at[b])
         incoming = ((b < z) & (z < lines - 1)) | ((b > z) & (z > 0))
-
-        @pl.when(incoming)
-        def _():
-            arrived(crecv.at[b], r_ch.at[b])
-            csend[b] = (pown[b] + precv[b].astype(jnp.float32) + crecv[b].astype(jnp.float32)).astype(csend.dtype)
-
-        @pl.when(jnp.logical_not(incoming))
-        def _():
-            csend[b] = (pown[b] + precv[b].astype(jnp.float32)).astype(csend.dtype)
-
-        @pl.when(b > z)
-        def _():
-            chain_copy(b, 1).start()
-
-        @pl.when(b < z)
-        def _():
-            chain_copy(b, 0).start()
-
-    def mixer_step(i, carry):
-        mixer(i)
-
-        @pl.when(i > 0)
-        def _():
-            chain(i - 1)
-
-        return carry
-
-    lax.fori_loop(0, lines, mixer_step, 0)
+        for c in range(pieces):
+            at = pl.ds(c * piece, piece)
+
+            @pl.when(incoming)
+            def _():
+                arrived(crecv.at[b, at, :], r_ch.at[b, c])
+                own = pown[b, at, :] + precv[b, at, :].astype(jnp.float32)
+                csend[b, at, :] = (own + crecv[b, at, :].astype(jnp.float32)).astype(csend.dtype)
+
+            @pl.when(jnp.logical_not(incoming))
+            def _():
+                own = pown[b, at, :] + precv[b, at, :].astype(jnp.float32)
+                csend[b, at, :] = own.astype(csend.dtype)
+
+            @pl.when(b > z)
+            def _():
+                chain_copy(b, 1, c).start()
+
+            @pl.when(b < z)
+            def _():
+                chain_copy(b, 0, c).start()
+
+    at_end = (z == 0) | (z == lines - 1)
+
+    @pl.when(at_end)
+    def _():
+        hidden_block(next_block(1))
+        rest_of_weights(2)
+        down_block(order(0))
+        chain(order(0))
+        for i in range(1, lines - 2):
+            from_above(i + 2)
+            from_below(i + 2)
+            hidden_block(next_block(i + 1))
+            down_block(order(i))
+            chain(order(i))
+        down_block(order(lines - 2))
+        chain(order(lines - 2))
+        down_block(z)
+
+    @pl.when(jnp.logical_not(at_end))
+    def _():
+        for i in range(3, lines):
+            from_above(i)
+            from_below(i)
+        for i in range(1, lines - 1):
+            hidden_block(next_block(i))
+        rest_of_weights(2)
+        for i in range(lines):
+            down_block(order(i))
+        for i in range(lines - 1):
+            chain(order(i))
+
     arrived(precv.at[z], r_pp.at[z])
     pown[z] = pown[z] + precv[z].astype(jnp.float32) + mid[tp].astype(jnp.float32)
-
-    @pl.when(z < lines - 1)
-    def _():
-        arrived(crecv.at[z], r_ch.at[z])
-        pown[z] = pown[z] + crecv[z].astype(jnp.float32)
-
-    @pl.when(z > 0)
-    def _():
-        arrived(crecv.at[lines], r_ch.at[lines])
-        pown[z] = pown[z] + crecv[lines].astype(jnp.float32)
-
-    out[...] = pown[z].astype(out.dtype)
+    for c in range(pieces):
+        at = pl.ds(c * piece, piece)
+
+        @pl.when(z < lines - 1)
+        def _():
+            arrived(crecv.at[z, at, :], r_ch.at[z, c])
+            pown[z, at, :] = pown[z, at, :] + crecv[z, at, :].astype(jnp.float32)
+
+        @pl.when(z > 0)
+        def _():
+            arrived(crecv.at[lines, at, :], r_ch.at[lines, c])
+            pown[z, at, :] = pown[z, at, :] + crecv[lines, at, :].astype(jnp.float32)
+
+        out[at, :] = pown[z, at, :].astype(out.dtype)
 
     for k in range(plane - 1):
         for a in range(6):
             qkv_copy(k, a).wait_send()
-        for d in range(lines):
-            for a in range(3):
-                w2_copy(k, d, a).wait_send()
+    for d in range(lines):
+        for a in range(3):
+            w2_copy(1, d, a).wait_send()
+            w2_copy(2, d, a).wait_send()
+            relay_copy(d, a).wait_send()
     for d in range(1, lines):
         for a in range(3):
             w1_copy(d, a).wait_send()
@@ -605,19 +692,23 @@
 
         @pl.when((b <= z) & (z < lines - 1))
         def _():
-            ag_copy(b, 1).wait_send()
+            for c in range(pieces):
+                ag_copy(b, 1, c).wait_send()
 
         @pl.when((b >= z) & (z > 0))
         def _():
-            ag_copy(b, 0).wait_send()
+            for c in range(pieces):
+                ag_copy(b, 0, c).wait_send()
 
         @pl.when(b > z)
         def _():
-            chain_copy(b, 1).wait_send()
+            for c in range(pieces):
+                chain_copy(b, 1, c).wait_send()
 
         @pl.when(b < z)
         def _():
-            chain_copy(b, 0).wait_send()
+            for c in range(pieces):
+                chain_copy(b, 0, c).wait_send()
 
 
 def fast_body(resid, query_one, key_one, query_two, key_two, values, mix_lambda, segments, head_gain,
@@ -629,13 +720,14 @@
     full = depth * plane * lines
     bf, f32 = jnp.bfloat16, jnp.float32
     sub = rows // 3
+    pieces = 2
     dma = pltpu.SemaphoreType.DMA
     anywhere = pl.BlockSpec(memory_space=pl.ANY)
     vmem = pl.BlockSpec(memory_space=pltpu.VMEM)
     smem = pl.BlockSpec(memory_space=pltpu.SMEM)
     flops = 6 * rows * plane * full * units + 2 * rows * full * half + 24 * rows * plane * rows * 5 * VD
     return pl.pallas_call(
-        functools.partial(layer_kernel, plane, lines, sub),
+        functools.partial(layer_kernel, plane, lines, sub, pieces),
         out_shape=jax.ShapeDtypeStruct((rows, half), bf),
         in_specs=[anywhere] * 6 + [smem, vmem, vmem, anywhere, vmem, anywhere, anywhere, anywhere],
         out_specs=vmem,
@@ -654,7 +746,7 @@
             pltpu.VMEM((full, units), bf),
             pltpu.VMEM((full, units), bf),
             pltpu.VMEM((units, full), bf),
-            pltpu.VMEM((rows, units), bf),
+            pltpu.VMEM((lines, rows, units), bf),
             pltpu.VMEM((lines, rows, half), f32),
             pltpu.VMEM((lines, rows, half), bf),
             pltpu.VMEM((lines, rows, half), bf),
@@ -662,13 +754,13 @@
             pltpu.VMEM((lines + 1, rows, half), bf),
             dma((plane - 1, 6)), dma((plane, 6)),
             dma((plane, 4)), dma((plane, 4)),
-            dma((lines - 1, 3)), dma((plane - 1, lines, 3)), dma((plane * lines, 3)),
+            dma((lines - 1, 3)), dma((2, lines, 3)), dma((lines, 3)), dma((plane * lines, 3)),
             dma((plane,)), dma((plane,)),
             dma((3,)), dma((3,)),
-            dma((lines, 2)), dma((lines,)),
+            dma((lines, 2, pieces)), dma((lines, pieces)),
             dma((lines,)), dma((lines,)),
             dma((lines,)), dma((lines,)),
-            dma((lines,)), dma((lines + 1,)),
+            dma((lines, pieces)), dma((lines + 1, pieces)),
             dma((11,)),
         ],
         compiler_params=pltpu.CompilerParams(

time: 227 us -> 200 us (0.88)
  Pallas kernels: 221 us -> 196 us
    pallas_call x1, Pallas kernels: 221 us -> 196 us  [fast_body(): pl.pallas_call(functools.partial(layer_kernel, plane, lines, sub, pieces)...]
where the time goes in v2:
time: 200 us
  Pallas kernels  196 us (98%)
  local copies, waits for them, and re-layouts  3.31 us (2%)
    pallas_call x1, Pallas kernels, fast_body(): pl.pallas_call(functools.partial(layer_kernel, plane, lines, sub, pieces)...  196 us

profile of v2, /device:TPU:0, one launch (start us, length us, event | category | flops | bytes accessed | tf_op | source)
XLA Modules:
  0.0 199.6 jit_solution(14025579910146864105)
XLA Ops:
  0.0 1.2 reshape.9.seg
  1.2 196.3 %layer.1 = bf16[384,1024]{1,0:T(8,128)(2,1)} custom-call(bf16[384,1024]{1,0:T(8,128)(2,1)} %resid.1, bf16[384,512]{1,0:T(8,128)(2,1)} %q_one.1, bf16[384,512]{1,0:T(8,128)(2,1)} %k_one.1, bf16[384,512]{1,0:T(8,128)(2,1)} %q_two.1, bf16[384,512]{1,0:T(8,128)(2,1)} %k_two.1, bf16[384,1024]{1,0:T(8,128)(2,1)} %vals.1, f32[4]{0:T(128)} %lam.1, ...), custom_call_target="tpu_custom_call" | custom-call | flops 34225520640 | bytes 3145728 | tf_op jit(solution)/shard_map/layer/pallas_call | solution.py:729
  197.5 2.1 %copy.16 = bf16[384,1024]{1,0:T(8,128)(2,1)} copy(bf16[384,1024]{1,0:T(8,128)(2,1)} %layer.1) | data formatting | bytes 1572864

commit v3 on v2

--- a/solution.py
+++ b/solution.py
@@ -239,12 +239,12 @@
 
     def qkv_copy(k, a):
         q = in_plane[k]
-        src = seg if a == 5 else qkv_src(a, q)
+        src = sb.at[plane + p] if a == 5 else qkv_src(a, q)
         return rdma(src, qkv_dst(a, p), s_qkv.at[k, a], r_qkv.at[p, a], (z * plane + q, tp))
 
     def halo_copy(block, a, own):
         if a == 3:
-            src = seg if own else sb.at[plane + block]
+            src = sb.at[plane + block]
             dst = sb.at[block]
         else:
             src = qkv_src(a, p) if own else kv_dst(a, plane + block)
@@ -305,8 +305,9 @@
     def local(src, dst, i):
         return pltpu.make_async_copy(src, dst, s_loc.at[i])
 
-    for a in (0, 1, 2, 5):
-        for k in range(plane - 1):
+    sb[plane + p] = seg[...].reshape(1, rows)
+    for k in range(plane - 1):
+        for a in (0, 1, 2, 5):
             qkv_copy(k, a).start()
     for k in range(plane - 1):
         for a in (3, 4):
@@ -331,7 +332,6 @@
         locals_.append(local(weight_src(z, a), weight_dst(sp, a), 7 + a))
     for c in locals_:
         c.start()
-    sb[plane + p] = seg[...]
     mg[tp] = mix_gain[...]
     rdma(mix_gain, mg.at[tp], s_pair.at[0], r_pair.at[0], partner).start()
 
@@ -536,25 +536,20 @@
     for d in range(1, lines):
         relay(d, 1)
         spread(d, 2)
+    inner = (z > 1) & (z < lines - 1)
     from_above(2)
-    from_below(1)
-    for c in locals_[7:]:
-        c.wait()
-    rest_of_weights(0)
-    rest_of_weights(1)
-    hidden_block(z)
-    for d in range(1, lines):
-        relay(d, 2)
-    hidden_block(next_block(0))
-    from_below(2)
+
+    @pl.when(jnp.logical_not(inner))
+    def _():
+        from_below(1)
 
     def rank(zz):
-        far = list(range(2, lines)) + [1]
-        back = [lines - 1 - b for b in far]
+        first = list(range(lines - 1, 0, -1))
+        last = list(range(lines - 2, -1, -1))
         travel = [
-            (far.index(b) + zz if b > zz else back.index(b) + lines - 1 - zz, b) for b in range(lines) if b != zz
+            (first.index(b) + zz if b > zz else last.index(b) + lines - 1 - zz, -b) for b in range(lines) if b != zz
         ]
-        return [b for _, b in sorted(travel)] + [zz]
+        return [-b for _, b in sorted(travel)] + [zz]
 
     def order(i):
         b = rank(0)[i]
@@ -562,6 +557,33 @@
             b = jnp.where(z == zz, rank(zz)[i], b)
         return b
 
+    relay(1, 2)
+
+    @pl.when(inner)
+    def _():
+        from_below(1)
+
+    for c in locals_[7:]:
+        c.wait()
+    rest_of_weights(0)
+    rest_of_weights(1)
+
+    @pl.when(z == lines - 1)
+    def _():
+        hidden_block(order(0))
+
+    @pl.when(z < lines - 1)
+    def _():
+        hidden_block(z)
+
+    for d in range(2, lines):
+        relay(d, 2)
+
+    @pl.when(inner)
+    def _():
+        from_below(2)
+
+    at_end = (z == 0) | (z == lines - 1)
     wide = half // 2
 
     def down_block(b):
@@ -586,10 +608,11 @@
             (sp + plane * (2 * to - 1), tp),
         )
 
-    def chain(b):
-        arrived(precv.at[b], r_pp.at[b])
+    def chain(b, lo=0, hi=pieces):
+        if lo == 0:
+            arrived(precv.at[b], r_pp.at[b])
         incoming = ((b < z) & (z < lines - 1)) | ((b > z) & (z > 0))
-        for c in range(pieces):
+        for c in range(lo, hi):
             at = pl.ds(c * piece, piece)
 
             @pl.when(incoming)
@@ -611,30 +634,51 @@
             def _():
                 chain_copy(b, 0, c).start()
 
-    at_end = (z == 0) | (z == lines - 1)
-
     @pl.when(at_end)
     def _():
-        hidden_block(next_block(1))
-        rest_of_weights(2)
-        down_block(order(0))
-        chain(order(0))
-        for i in range(1, lines - 2):
-            from_above(i + 2)
-            from_below(i + 2)
-            hidden_block(next_block(i + 1))
+        for i in range(3, lines):
+            from_above(i)
+        for i in range(lines - 1):
+            if i > 0:
+                from_below(i + 1)
+            if i == 0:
+
+                @pl.when(z == 0)
+                def _():
+                    hidden_block(order(0))
+
+                rest_of_weights(2)
+            if i > 0:
+                hidden_block(order(i))
             down_block(order(i))
-            chain(order(i))
-        down_block(order(lines - 2))
-        chain(order(lines - 2))
+            if i == 0:
+                chain(order(i), 0, pieces // 2)
+
+                @pl.when(z == 0)
+                def _():
+                    chain(order(i), pieces // 2)
+
+            else:
+                chain(order(i))
+
+        @pl.when(z > 0)
+        def _():
+            chain(order(0), pieces // 2)
+            hidden_block(z)
+
         down_block(z)
 
+
     @pl.when(jnp.logical_not(at_end))
     def _():
+        @pl.when(jnp.logical_not(inner))
+        def _():
+            from_below(2)
+
         for i in range(3, lines):
             from_above(i)
             from_below(i)
-        for i in range(1, lines - 1):
+        for i in range(lines - 1):
             hidden_block(next_block(i))
         rest_of_weights(2)
         for i in range(lines):
@@ -720,7 +764,7 @@
     full = depth * plane * lines
     bf, f32 = jnp.bfloat16, jnp.float32
     sub = rows // 3
-    pieces = 2
+    pieces = 8
     dma = pltpu.SemaphoreType.DMA
     anywhere = pl.BlockSpec(memory_space=pl.ANY)
     vmem = pl.BlockSpec(memory_space=pltpu.VMEM)
@@ -768,7 +812,7 @@
         ),
         cost_estimate=pl.CostEstimate(flops=flops, bytes_accessed=2 * full * units, transcendentals=0),
         name="layer",
-    )(resid, query_one, key_one, query_two, key_two, values, mix_lambda, segments.reshape(1, rows),
+    )(resid, query_one, key_one, query_two, key_two, values, mix_lambda, segments,
       head_gain.reshape(1, VD), out_weight, mixer_gain.reshape(1, half), gate_weight, up_weight, down_weight)
 
 

time: 200 us -> 199 us (level)
  no operation moved by 1% of the time
where the time goes in v3:
time: 199 us; the launch traced here: 198 us
  Pallas kernels  196 us (98%)
  local copies, waits for them, and re-layouts  2.06 us (1%)
    pallas_call x1, Pallas kernels, fast_body(): pl.pallas_call(functools.partial(layer_kernel, plane, lines, sub, pieces)...  196 us

profile of v3, /device:TPU:0, one launch (start us, length us, event | category | flops | bytes accessed | tf_op | source)
XLA Modules:
  0.0 198.3 jit_solution(13124272137356137422)
XLA Ops:
  0.0 196.3 %layer.1 = bf16[384,1024]{1,0:T(8,128)(2,1)} custom-call(bf16[384,1024]{1,0:T(8,128)(2,1)} %resid.1, bf16[384,512]{1,0:T(8,128)(2,1)} %q_one.1, bf16[384,512]{1,0:T(8,128)(2,1)} %k_one.1, bf16[384,512]{1,0:T(8,128)(2,1)} %q_two.1, bf16[384,512]{1,0:T(8,128)(2,1)} %k_two.1, bf16[384,1024]{1,0:T(8,128)(2,1)} %vals.1, f32[4]{0:T(128)} %lam.1, s32[384]{0:T(512)} %seg.1, ...), custom_call_target="tpu_custom_call" | custom-call | flops 34225520640 | bytes 3145728 | tf_op jit(solution)/shard_map/layer/pallas_call | solution.py:773
  196.3 2.1 %copy.16 = bf16[384,1024]{1,0:T(8,128)(2,1)} copy(bf16[384,1024]{1,0:T(8,128)(2,1)} %layer.1) | data formatting | bytes 1572864
